TPU v7x, 256 devices: a whole 4x4x8 slice. The times are simulated.
256 devices in a mesh: ep: 64 (over z, x, core), tp: 4 (over y).
Axes of the slice: x: 4, y: 4, z: 8, core: 2. Of those that a mesh axis runs over, the one named last changes fastest.
Arguments:
- gate_branch: bfloat16 [32768, 2048], P(('ep', 'tp')), may hold values from -8 to 8
- rec_branch: bfloat16 [32768, 2048], P(('ep', 'tp')), may hold values from -6 to 6
- conv_weight: float32 [4, 2048], replicated, may hold values from -3 to 3
- gate_a: bfloat16 [8, 256, 256], replicated, may hold values from -0.375 to 0.375
- gate_x: bfloat16 [8, 256, 256], replicated, may hold values from -0.375 to 0.375
- decay_param: float32 [2048], replicated, as said below
- decay_shift: float32 [32768], P(('ep', 'tp')), may hold values from -0.6 to 0
- tokens: bfloat16 [32768, 2048], P(('ep', 'tp')), may hold values from -6 to 6
- routes: int32 [32768, 2], P(('ep', 'tp')), may hold values from 0 to 63, all different within a row; in each aligned block of 128 rows (0 to 127, 128 to 255, ...) at most 5 rows name the same one
- route_weight: float32 [32768, 2], P(('ep', 'tp')), may hold values from 0.1 to 0.9
- norm_gain: float32 [2048], replicated, may hold values from 0.1 to 1.9
- w_gate: bfloat16 [64, 2048, 3584], P('ep', None, 'tp'), may hold values from -0.125 to 0.125
- w_up: bfloat16 [64, 2048, 3584], P('ep', None, 'tp'), may hold values from -0.125 to 0.125
- w_down: bfloat16 [64, 3584, 2048], P('ep', 'tp'), may hold values from -0.09375 to 0.09375
Outputs:
- mixed_out: bfloat16 [32768, 2048], P(('ep', 'tp'))
- expert_out: bfloat16 [32768, 2048], P(('ep', 'tp'))
Inputs may be any that keep to these rules, and one draw needn't show every extreme that they name: `routes`: in each aligned block of 128 rows (the rows of one device) no expert is named more than 5 times, and some block names some expert exactly 5 times; the experts of one row differ. 8 softplus(-decay_param) lies between 0.2 / 32768 and 0.07.
All inputs are finite; a program needn't handle non-finite values.
Results may differ from a plain program's by a relative error of at most 0.012.
Values may be sent and summed in bfloat16 or wider, within the bound.
A program may use at most 128 MiB of HBM per device.

v0:
```python
import math
import jax
import jax.numpy as jnp
from jax import lax
from jax.sharding import Mesh
from jax.sharding import PartitionSpec as P

EP_TP = ("ep_0", "ep_1", "ep_2", "tp")
EP = ("ep_0", "ep_1", "ep_2")
EPSILON = 1e-05


def passed_along(block, axis, distance):
    devices = range(lax.axis_size(axis))
    route = [(i - distance, i) for i in devices if i - distance in devices]
    return lax.ppermute(block, axis, route)


def neutral_like(array, identity):
    return jax.tree.map(
        lambda part, zero: jnp.zeros_like(part) + jnp.asarray(zero, part.dtype), array, identity
    )


def gathered_once(array, axis):
    leaves = jax.tree.leaves(array)
    sequence = sorted(range(len(leaves)), key=lambda k: -leaves[k].size)
    width = (1, *leaves[sequence[0]].shape)[-1]
    lines = [
        jnp.pad(leaves[k].reshape(-1), (0, -leaves[k].size % width)).reshape(-1, width)
        for k in sequence
    ]
    both, at, found = (lax.all_gather(jnp.concatenate(lines), axis), 0, {})
    for k, line in zip(sequence, lines):
        piece = both[:, at : at + len(line)].reshape(len(both), -1)
        found[k] = piece[:, : leaves[k].size].reshape(-1, *leaves[k].shape)
        at += len(line)
    numbers = iter(range(len(leaves)))
    return jax.tree.map(lambda _: found[next(numbers)], array)


def carried_in(array, axes, combine, identity):
    before = start = neutral_like(array, identity)
    subtotal = array
    for axis in reversed(axes):
        length, here = (lax.axis_size(axis), lax.axis_index(axis))
        pieces = gathered_once(subtotal, axis)
        inside, subtotal = (start, start)
        for k in range(length):
            passed = k < here
            subtotal = combine(subtotal, jax.tree.map(lambda part: part[k], pieces))
            inside = jax.tree.map(lambda new, old: jnp.where(passed, new, old), subtotal, inside)
        before = combine(inside, before)
    return before


def pair_combine(earlier, later):
    return (earlier[0] * later[0], later[0] * earlier[1] + later[1])


def short_conv(previous, current, conv_weight):
    tap_count = conv_weight.shape[0]
    row_count = current.shape[0]
    padded = jnp.concatenate([previous, current], 0)
    summed = jnp.zeros(current.shape, jnp.float32)
    for tap_index in range(tap_count):
        summed = summed + conv_weight[tap_index] * padded[tap_index : tap_index + row_count].astype(
            jnp.float32
        )
    return summed.astype(jnp.bfloat16)


def mixer_gates(conv_rows, gate_a, gate_x, decay_rate, shift_rows):
    row_count, width_all = conv_rows.shape
    block_count, block_width = (gate_a.shape[0], gate_a.shape[1])
    split_rows = conv_rows.reshape(row_count, block_count, block_width)
    pre_a = jnp.einsum("rnc,ncd->rnd", split_rows, gate_a, preferred_element_type=jnp.float32)
    pre_x = jnp.einsum("rnc,ncd->rnd", split_rows, gate_x, preferred_element_type=jnp.float32)
    recur_gate = jax.nn.sigmoid(pre_a.reshape(row_count, width_all))
    input_gate = jax.nn.sigmoid(pre_x.reshape(row_count, width_all))
    log_a = -decay_rate[None, :] * recur_gate + shift_rows[:, None]
    drive = jnp.sqrt(-jnp.expm1(2.0 * log_a)) * input_gate * conv_rows.astype(jnp.float32)
    return (log_a, drive)


def blocked_recurrence(decay, drive):
    row_count, width_all = decay.shape
    group = math.gcd(row_count, 8)
    block_count = row_count // group
    decay_blocks = decay.reshape(block_count, group, width_all)
    drive_blocks = drive.reshape(block_count, group, width_all)
    factors = [decay_blocks[:, 0]]
    states = [drive_blocks[:, 0]]
    for inner in range(1, group):
        factors.append(factors[-1] * decay_blocks[:, inner])
        states.append(decay_blocks[:, inner] * states[-1] + drive_blocks[:, inner])
    factor_inner = jnp.stack(factors, 1)
    state_inner = jnp.stack(states, 1)

    def carry_step(carried, totals):
        return (pair_combine(carried, totals), carried)

    start = (jnp.ones((width_all,), jnp.float32), jnp.zeros((width_all,), jnp.float32))
    _, before = lax.scan(carry_step, start, (factors[-1], states[-1]))
    factor_all = factor_inner * before[0][:, None, :]
    state_all = state_inner + factor_inner * before[1][:, None, :]
    return (factor_all.reshape(row_count, width_all), state_all.reshape(row_count, width_all))


def layer_scale(rows_in, norm_gain):
    values = rows_in.astype(jnp.float32)
    center = jnp.mean(values, -1, keepdims=True)
    spread = jnp.mean(jnp.square(values - center), -1, keepdims=True)
    return ((values - center) * lax.rsqrt(spread + EPSILON) * norm_gain).astype(jnp.bfloat16)


def slot_numbers(routes, block_rows, expert_count):
    row_count, top_count = routes.shape
    onehot = (routes[:, :, None] == jnp.arange(expert_count, dtype=jnp.int32)).astype(jnp.int32)
    ranked = (
        jnp.cumsum(
            onehot.reshape(row_count // block_rows, block_rows * top_count, expert_count), axis=1
        )
        - 1
    )
    return jnp.sum(ranked.reshape(row_count, top_count, expert_count) * onehot, -1)


def expert_hidden(rows_in, gate_part, up_part):
    return (
        jax.nn.silu(jnp.dot(rows_in, gate_part, preferred_element_type=jnp.float32))
        * jnp.dot(rows_in, up_part, preferred_element_type=jnp.float32)
    ).astype(jnp.bfloat16)


def shards(
    gate_branch,
    rec_branch,
    conv_weight,
    gate_a,
    gate_x,
    decay_param,
    decay_shift,
    tokens,
    routes,
    route_weight,
    norm_gain,
    w_gate,
    w_up,
    w_down,
):
    tap_count = conv_weight.shape[0]
    row_count, width_all = rec_branch.shape
    previous = passed_along(rec_branch[row_count - (tap_count - 1) :], EP_TP, 1)
    conv_rows = short_conv(previous, rec_branch, conv_weight)
    decay_rate = 8.0 * jax.nn.softplus(-decay_param)
    log_a, drive = mixer_gates(conv_rows, gate_a, gate_x, decay_rate, decay_shift)
    factor, local_state = blocked_recurrence(jnp.exp(log_a), drive)
    identity = (jnp.ones((width_all,), jnp.float32), jnp.zeros((width_all,), jnp.float32))
    carried = carried_in((factor[-1], local_state[-1]), EP_TP, pair_combine, identity)
    states = local_state + factor * carried[1][None, :]
    mixed_out = (states * jax.nn.gelu(gate_branch.astype(jnp.float32), approximate=True)).astype(
        jnp.bfloat16
    )
    ep_count = lax.axis_size(EP)
    block_rows, top_count = routes.shape
    capacity = max(2, block_rows * top_count * 5 // (4 * ep_count))
    normed = layer_scale(tokens, norm_gain)
    slots = slot_numbers(routes, block_rows, ep_count)
    row_ids = jnp.broadcast_to(jnp.arange(block_rows, dtype=jnp.int32)[:, None], routes.shape)
    flat = routes * capacity + slots
    table = jnp.full((ep_count * capacity,), block_rows, jnp.int32)
    table = table.at[flat.reshape(-1)].set(row_ids.reshape(-1))
    outgoing = jnp.take(normed, table, axis=0, mode="fill", fill_value=0)
    outgoing = outgoing.reshape(ep_count, capacity, width_all)
    arrived = lax.all_to_all(outgoing, EP, split_axis=0, concat_axis=0, tiled=True)
    hidden = expert_hidden(
        lax.all_gather(arrived.reshape(-1, width_all), "tp", axis=0, tiled=True), w_gate[0], w_up[0]
    )
    route_out = lax.psum_scatter(
        jnp.dot(hidden, w_down[0], preferred_element_type=jnp.float32).astype(jnp.bfloat16),
        "tp",
        scatter_dimension=0,
        tiled=True,
    )
    returned = lax.all_to_all(
        route_out.reshape(ep_count, capacity, width_all),
        EP,
        split_axis=0,
        concat_axis=0,
        tiled=True,
    )
    returned = returned.reshape(ep_count * capacity, width_all)
    picked = jnp.take(returned, flat.reshape(-1), axis=0).astype(jnp.float32)
    picked = picked.reshape(block_rows, top_count, width_all)
    expert_out = jnp.sum(picked * route_weight[:, :, None], axis=1).astype(jnp.bfloat16)
    return (mixed_out, expert_out)


def solution(mesh):
    split = Mesh(mesh.devices.reshape(8, 4, 2, mesh.shape["tp"]), ("ep_0", "ep_1", "ep_2", "tp"))
    return jax.shard_map(
        shards,
        mesh=split,
        in_specs=(
            P(EP_TP, None),
            P(EP_TP, None),
            P(),
            P(),
            P(),
            P(),
            P(EP_TP),
            P(EP_TP, None),
            P(EP_TP, None),
            P(EP_TP, None),
            P(),
            P(EP, None, "tp"),
            P(EP, None, "tp"),
            P(EP, "tp", None),
        ),
        out_specs=(P(EP_TP, None), P(EP_TP, None)),
        check_vma=False,
    )
```

profile of v0, /device:TPU:2, one launch (start us, length us, event | category | flops | bytes accessed | tf_op | source)
XLA Modules:
  0.0 314.5 jit_solution(11399140220905587292)
XLA Ops:
  7.2 0.9 copy.64
  8.3 0.6 reduce-window.6
  9.8 0.7 compare_and_fusion.1
  10.9 1.4 scatter_custom_fusion
  12.4 1.2 convert_reduce_fusion
  13.6 1.3 fusion.14
  14.9 1.4 fusion.16
  16.3 3.0 gather_fusion
  19.3 2.4 gather.13
  22.1 63.1 %all_to_all.10 = bf16[64,5,2048]{2,1,0:T(8,128)(2,1)S(1)} all-to-all(bf16[64,5,2048]{2,1,0:T(8,128)(2,1)S(1)} %broadcast_select_fusion.2), channel_id=1, replica_groups=mesh['ep_0'=8,'ep_1'=4,'ep_2'=2,'tp'=4] {'ep_0','ep_1','ep_2'}, dimensions={0} | all-to-all | bytes 2621440 | tf_op jit(solution)/shard_map/all_to_all | solution.py:176
  85.2 1.4 reshape.838
  86.7 0.8 slice.280
  87.8 3.7 %collective-permute-start = (bf16[3,2048]{0,1:T(8,128)(2,1)S(1)}, bf16[3,2048]{0,1:T(8,128)(2,1)S(1)}, u32[]{:S(2)}, u32[]{:S(2)}) collective-permute-start(bf16[3,2048]{0,1:T(8,128)(2,1)S(1)} %copy.55), channel_id=1, source_target_pairs={{0,1},{1,2},{2,3},{3,4},{4,5},{5,6},{6,7},{7,8},{8,9},{9,10},{10,1... | collective-permute-start | bytes 36872 | tf_op jit(solution)/shard_map/ppermute | solution.py:16
  91.5 0.6 pad_clamp_fusion
  92.1 1.3 copy.56
  93.6 0.7 copy.69
  94.3 0.7 copy.71
  95.1 12.4 %collective-permute-done = bf16[3,2048]{0,1:T(8,128)(2,1)S(1)} collective-permute-done((bf16[3,2048]{0,1:T(8,128)(2,1)S(1)}, bf16[3,2048]{0,1:T(8,128)(2,1)S(1)}, u32[]{:S(2)}, u32[]{:S(2)}) %collective-permute-start) | collective-permute-done | bytes 12320 | tf_op jit(solution)/shard_map/ppermute | solution.py:16
  107.5 2.1 add_convert_fusion
  109.6 0.8 copy-done.2
  110.4 0.5 fusion.11
  111.2 0.6 copy.63
  111.8 2.9 fusion.7
  114.7 1.5 copy.61
  116.3 3.0 fusion.24
  119.2 1.6 copy.62
  121.2 2.2 slice_add_fusion
  123.4 2.8 stack.4
  126.2 0.7 slice_multiply_fusion
  127.0 2.6 stack.5
  129.5 18.4 %all-gather.10.cloned.1.call-done = bf16[1280,2048]{1,0:T(8,128)(2,1)} async-done(((bf16[320,2048]{1,0:T(8,128)(2,1)}), bf16[1280,2048]{1,0:T(8,128)(2,1)}) %all-gather.10.cloned.1.call-update) | async-done | bytes 5242896 | tf_op jit(solution)/shard_map/all_gather | solution.py:178
  148.0 9.9 %fusion.2 = f32[1280,896]{1,0:T(8,128)} fusion(bf16[1280,2048]{1,0:T(8,128)(2,1)} %all-gather.10.cloned.1.call-done, bf16[1,2048,896]{2,1,0:T(8,128)(2,1)} %param.27), kind=kOutput, calls=%fused_computation.12 | convolution fusion | flops 4697620480 | bytes 13500416 | tf_op jit(solution)/shard_map/dot_general | solution.py:131
  157.9 17.6 %convolution_convert_fusion = bf16[1280,2048]{1,0:T(8,128)(2,1)} fusion(bf16[1,896,2048]{2,1,0:T(8,128)(2,1)} %param.29, f32[1280,896]{1,0:T(8,128)} %fusion.2, bf16[1280,2048]{1,0:T(8,128)(2,1)} %all-gather.10.cloned.1.call-done, bf16[1,2048,896]{2,1,0:T(8,128)(2,1)} %param.28), kind=kOutput, calls=%fused_computation.8 | convolution fusion | flops 9404743680 | bytes 22413312 | tf_op jit(solution)/shard_map/dot_general | solution.py:181
  175.6 0.8 copy-done.5
  176.4 7.8 %while.17 = (s32[]{:T(128)}, f32[2048]{0:T(1024)S(1)}, f32[2048]{0:T(1024)S(1)}, f32[16,2048]{1,0:T(8,128)S(1)}, f32[16,2048]{1,0:T(8,128)S(1)}, /*index=5*/f32[...) while((s32[]{:T(128)}, f32[2048]{0:T(1024)S(1)}, f32[2048]{0:T(1024)S(1)}, ...), condition=%wide.region_1.2_spmd.clone, body=%wide.region_0.1_spmd.clone.sunk | while | flops 10243 | bytes 131187 | solution.py:104
  184.2 1.5 multiply_bitcast_fusion
  185.8 12.5 %all-gather.4 = f32[4,2,2048]{2,1,0:T(2,128)S(1)} all-gather(f32[1,2,2048]{2,1,0:T(2,128)S(1)} %maximum_bitcast_fusion), channel_id=2, replica_groups=mesh['ep_0'=8,'ep_1'=4,'ep_2'=2,'tp'=4] {'tp'}, dimensions={0}, use_global_device_ids=true | all-gather | bytes 81920 | tf_op jit(solution)/shard_map/all_gather | solution.py:33
  198.4 1.8 all-gather.5
  200.3 11.9 %all-gather.6 = f32[4,2,2048]{2,1,0:T(2,128)S(1)} all-gather(f32[1,2,2048]{2,1,0:T(2,128)S(1)} %maximum_bitcast_fusion.2), channel_id=4, replica_groups=mesh['ep_0'=8,'ep_1'=4,'ep_2'=2,'tp'=4] {'ep_1'}, dimensions={0}, use_global_device_ids=true | all-gather | bytes 81920 | tf_op jit(solution)/shard_map/all_gather | solution.py:33
  212.2 24.6 %all-gather.7 = f32[8,2,2048]{2,1,0:T(2,128)S(1)} all-gather(f32[1,2,2048]{2,1,0:T(2,128)S(1)} %maximum_bitcast_fusion.3), channel_id=5, replica_groups=mesh['ep_0'=8,'ep_1'=4,'ep_2'=2,'tp'=4] {'ep_0'}, dimensions={0}, use_global_device_ids=true | all-gather | bytes 147456 | tf_op jit(solution)/shard_map/all_gather | solution.py:33
  236.8 3.4 %reshape.839 = bf16[64,5,2048]{2,1,0:T(8,128)(2,1)} reshape(bf16[320,2048]{1,0:T(8,128)(2,1)} %reduce-scatter.2.cloned.1.call-done) | data formatting | bytes 2621440 | tf_op jit(solution)/shard_map/reshape | solution.py:187
  240.3 6.4 %all-to-all-start.1 = ((bf16[64,5,2048]{2,1,0:T(8,128)(2,1)}), bf16[64,5,2048]{2,1,0:T(8,128)(2,1)}, u32[]{:S(2)}, u32[]{:S(2)}) async-start(bf16[64,5,2048]{2,1,0:T(8,128)(2,1)} %reshape.839), calls=%async_computation.2 | async-start | bytes 4194304 | tf_op jit(solution)/shard_map/all_to_all | solution.py:186
  247.0 1.3 fusion.23
  248.2 49.6 %all-to-all-done.1 = bf16[64,5,2048]{2,1,0:T(8,128)(2,1)} async-done(((bf16[64,5,2048]{2,1,0:T(8,128)(2,1)}), bf16[64,5,2048]{2,1,0:T(8,128)(2,1)}, u32[]{:S(2)}, u32[]{:S(2)}) %all-to-all-start.1) | async-done | bytes 1310752 | tf_op jit(solution)/shard_map/all_to_all | solution.py:186
  297.8 2.6 reshape.840
  300.4 1.6 gather_fusion.1
  302.0 0.7 gather.15
  302.8 4.9 %multiply_reduce_fusion = bf16[128,2048]{1,0:T(8,128)(2,1)} fusion(bf16[128,2,2048]{2,1,0:T(2,128)(2,1)S(1)} %gather.15, pred[128,2]{1,0:T(8,128)(4,1)S(1)} %copy-done.7, f32[128,2]{1,0:T(8,128)S(1)} %copy-done.4), kind=kLoop, calls=%fused_computation.14 | loop fusion | flops 1835008 | bytes 1574144 | tf_op jit(solution)/shard_map/reduce_sum | solution.py:196
  (142 shorter events, 10.8 us)
Async XLA Ops:
  7.2 103.2 %copy-start = (bf16[8,256,256]{2,1,0:T(8,128)(2,1)S(1)}, bf16[8,256,256]{2,1,0:T(8,128)(2,1)}, u32[]{:S(2)}) copy-start(bf16[8,256,256]{2,1,0:T(8,128)(2,1)} %param.19) | copy-start | bytes 3145732
  7.2 140.8 %all-gather.10.cloned.1.call-start = ((), (), s32[]{:S(2)}) async-start(), calls=%async_computation.3 | async-start | bytes 6553600 | tf_op jit(solution)/shard_map/all_gather | solution.py:178
  85.2 6.3 %copy-start.9 = (f32[2048]{0:T(1024)S(1)}, f32[2048]{0:T(1024)}, u32[]{:S(2)}) copy-start(f32[2048]{0:T(1024)} %param.21) | copy-start | bytes 24580
  85.2 6.3 %copy-start.8 = (f32[4,2048]{1,0:T(4,128)S(1)}, f32[4,2048]{1,0:T(4,128)}, u32[]{:S(2)}) copy-start(f32[4,2048]{1,0:T(4,128)} %param.18) | copy-start | bytes 98308
  85.2 8.3 %copy-start.10 = (f32[128]{0:T(128)S(1)}, f32[128]{0:T(128)}, u32[]{:S(2)}) copy-start(f32[128]{0:T(128)} %param.22) | copy-start | bytes 1540
  85.2 9.1 %copy-start.11 = (f32[128,2]{0,1:T(2,128)S(1)}, f32[128,2]{0,1:T(2,128)}, u32[]{:S(2)}) copy-start(f32[128,2]{0,1:T(2,128)} %param.25) | copy-start | bytes 3076
  86.6 150.2 %reduce-scatter.2.cloned.1.call-start = ((), (), s32[]{:S(2)}) async-start(), calls=%async_computation.4 | async-start | bytes 6553600 | tf_op jit(solution)/shard_map/reduce_scatter | solution.py:180
  87.8 19.7 %collective-permute-start = (bf16[3,2048]{0,1:T(8,128)(2,1)S(1)}, bf16[3,2048]{0,1:T(8,128)(2,1)S(1)}, u32[]{:S(2)}, u32[]{:S(2)}) collective-permute-start(bf16[3,2048]{0,1:T(8,128)(2,1)S(1)} %copy.55), channel_id=1, source_target_pairs={{0,1},{1,2},{2,3},{3,4},{4,5},{5,6},{6,7},{7,8},{8,9},{9,10},{10,1... | collective-permute-start | bytes 36872 | tf_op jit(solution)/shard_map/ppermute | solution.py:16
  109.6 0.8 copy-start.2
  175.5 0.9 copy-start.5
  175.5 1.0 copy-start.6
  236.8 10.2 %copy-start.3 = (bf16[128,2048]{1,0:T(8,128)(2,1)S(1)}, bf16[128,2048]{1,0:T(8,128)(2,1)}, u32[]{:S(2)}) copy-start(bf16[128,2048]{1,0:T(8,128)(2,1)} %param.16) | copy-start | bytes 1572868
  240.3 57.5 %all-to-all-start.1 = ((bf16[64,5,2048]{2,1,0:T(8,128)(2,1)}), bf16[64,5,2048]{2,1,0:T(8,128)(2,1)}, u32[]{:S(2)}, u32[]{:S(2)}) async-start(bf16[64,5,2048]{2,1,0:T(8,128)(2,1)} %reshape.839), calls=%async_computation.2 | async-start | bytes 4194304 | tf_op jit(solution)/shard_map/all_to_all | solution.py:186
  300.3 2.4 copy-start.4
  300.3 2.4 copy-start.7
  300.4 7.3 %copy-start.1 = (bf16[8,256,256]{2,1,0:T(8,128)(2,1)S(1)}, bf16[8,256,256]{2,1,0:T(8,128)(2,1)}, u32[]{:S(2)}) copy-start(bf16[8,256,256]{2,1,0:T(8,128)(2,1)} %param.19) | copy-start | bytes 3145732
Sparse Core Ops, SparseCore 0:
  86.8 61.1 all-gather.9
  175.6 53.6 reduce-scatter.1
where the time goes:
time: 316 us; the launch traced here: 315 us
  blocking collectives  114 us (36%)
  waiting for transfers between devices  80.4 us (25%)
  local copies, waits for them, and re-layouts  41.1 us (13%)
  matrix products  30.9 us (10%)
  other arithmetic  22.8 us (7%)
  between operations  14.6 us (5%)
  starting transfers between devices  10.1 us (3%)
    all_to_all x1, blocking collectives, shards(): lax.all_to_all(outgoing, EP, split_axis=0, concat_axis=0, tiled=True)  63.1 us
    all_gather x4, blocking collectives, gathered_once(): both, at, found = (lax.all_gather(jnp.concatenate(lines), axis), 0, {})  50.8 us
    all_to_all x1, waiting for transfers between devices, shards(): lax.all_to_all(route_out.reshape(ep_count, capacity, width_all), EP, spli...  49.6 us
    all_gather x1, waiting for transfers between devices, shards(): lax.all_gather(arrived.reshape(-1, width_all), 'tp', axis=0, tiled=True)  18.4 us
    dot_general x1, matrix products, shards(): jnp.dot(hidden, w_down[0], preferred_element_type=jnp.float32)  17.6 us
    ppermute x1, waiting for transfers between devices, passed_along(): return lax.ppermute(block, axis, route)  12.4 us
    dot_general x1, matrix products, expert_hidden(): jnp.dot(rows_in, gate_part, preferred_element_type=jnp.float32)  9.94 us
    dynamic_update_slice x32, local copies, waits for them, and re-layouts, blocked_recurrence(): _, before = lax.scan(carry_step, start, (factors[-1], states[-1]))  6.55 us
  transfers between devices with their start and end apart: 4, of which 3 were waited for; matrix products, arithmetic and copies ran while one was open for 11% of the time, Pallas kernels for 0%

commit v1 on v0

--- a/solution.py
+++ b/solution.py
@@ -8,6 +8,24 @@
 EP_TP = ("ep_0", "ep_1", "ep_2", "tp")
 EP = ("ep_0", "ep_1", "ep_2")
 EPSILON = 1e-05
+
+
+def gather_around(shard, axis, dim):
+    ways, here, step = (lax.axis_size(axis), lax.axis_index(axis), shard.shape[dim])
+    shape = [n * ways if d == dim else n for d, n in enumerate(shard.shape)]
+    full = lax.dynamic_update_slice_in_dim(
+        jnp.zeros(shape, shard.dtype), shard, here * step, axis=dim
+    )
+    going_up = going_down = shard
+    for far in range(1, ways // 2 + 1):
+        going_up = lax.ppermute(going_up, axis, [(d, (d + 1) % ways) for d in range(ways)])
+        full = lax.dynamic_update_slice_in_dim(full, going_up, (here - far) % ways * step, axis=dim)
+        if 2 * far < ways:
+            going_down = lax.ppermute(going_down, axis, [(d, (d - 1) % ways) for d in range(ways)])
+            full = lax.dynamic_update_slice_in_dim(
+                full, going_down, (here + far) % ways * step, axis=dim
+            )
+    return full
 
 
 def passed_along(block, axis, distance):
@@ -175,7 +193,7 @@
     outgoing = outgoing.reshape(ep_count, capacity, width_all)
     arrived = lax.all_to_all(outgoing, EP, split_axis=0, concat_axis=0, tiled=True)
     hidden = expert_hidden(
-        lax.all_gather(arrived.reshape(-1, width_all), "tp", axis=0, tiled=True), w_gate[0], w_up[0]
+        gather_around(arrived.reshape(-1, width_all), "tp", 0), w_gate[0], w_up[0]
     )
     route_out = lax.psum_scatter(
         jnp.dot(hidden, w_down[0], preferred_element_type=jnp.float32).astype(jnp.bfloat16),

time: 316 us -> 324 us (1.025)
  blocking collectives: 114 us -> 53.9 us
  waiting for transfers between devices: 80.4 us -> 110 us
  starting transfers between devices: 10.1 us -> 29.3 us
  local copies, waits for them, and re-layouts: 41.1 us -> 56.3 us
  other arithmetic: 22.8 us -> 28.8 us
    all_to_all x1 -> x0, blocking collectives: 63.1 us -> none  [shards(): lax.all_to_all(outgoing, EP, split_axis=0, concat_axis=0, tiled=True)]
    ppermute x0 -> x3, waiting for transfers between devices: none -> 30.1 us  [the longest x2 30.1 us: gather_around(): lax.ppermute(going_up, axis, [(d, (d + 1) % ways) for d in range(ways)])]
    all_to_all x0 -> x1, waiting for transfers between devices: none -> 19 us  [shards(): lax.all_to_all(outgoing, EP, split_axis=0, concat_axis=0, tiled=True)]
    all_gather x1 -> x0, waiting for transfers between devices: 18.4 us -> none  [shards(): lax.all_gather(arrived.reshape(-1, width_all), 'tp', axis=0, tiled=True)]
    all_to_all x0 -> x1, starting transfers between devices: none -> 12.1 us  [shards(): lax.all_to_all(outgoing, EP, split_axis=0, concat_axis=0, tiled=True)]
    dynamic_update_slice x0 -> x4, local copies, waits for them, and re-layouts: none -> 4.71 us  [the longest x2 3.08 us: gather_around(): lax.dynamic_update_slice_in_dim(full, going_up, (here - far) % ways * ste...]
    div x4, local copies, waits for them, and re-layouts: 2.65 us -> 7.05 us  [mixer_gates(): recur_gate = jax.nn.sigmoid(pre_a.reshape(row_count, width_all))]
    ppermute x0 -> x3, starting transfers between devices: none -> 3.88 us  [the longest x1 2 us: gather_around(): lax.ppermute(going_down, axis, [(d, (d - 1) % ways) for d in range(ways)])]
  transfers between devices with their start and end apart: 4 -> 7, of which waited for: 3 -> 5; matrix products, arithmetic and copies ran while one was open for 11% -> 16% of each run, Pallas kernels for 0% -> 0%
where the time goes in v1:
time: 324 us; the launch traced here: 323 us
  waiting for transfers between devices  110 us (34%)
  local copies, waits for them, and re-layouts  56.3 us (17%)
  blocking collectives  53.9 us (17%)
  starting transfers between devices  29.3 us (9%)
  matrix products  29 us (9%)
  other arithmetic  28.8 us (9%)
  between operations  14.6 us (5%)
    all_gather x4, blocking collectives, gathered_once(): both, at, found = (lax.all_gather(jnp.concatenate(lines), axis), 0, {})  53.9 us
    all_to_all x1, waiting for transfers between devices, shards(): lax.all_to_all(route_out.reshape(ep_count, capacity, width_all), EP, spli...  49.6 us
    ppermute x2, waiting for transfers between devices, gather_around(): lax.ppermute(going_up, axis, [(d, (d + 1) % ways) for d in range(ways)])  30.1 us
    all_to_all x1, waiting for transfers between devices, shards(): lax.all_to_all(outgoing, EP, split_axis=0, concat_axis=0, tiled=True)  19 us
    dot_general x1, matrix products, shards(): jnp.dot(hidden, w_down[0], preferred_element_type=jnp.float32)  17.5 us
    all_to_all x1, starting transfers between devices, shards(): lax.all_to_all(outgoing, EP, split_axis=0, concat_axis=0, tiled=True)  12.1 us
    ppermute x1, waiting for transfers between devices, passed_along(): return lax.ppermute(block, axis, route)  11.4 us
    all_to_all x1, starting transfers between devices, shards(): lax.all_to_all(route_out.reshape(ep_count, capacity, width_all), EP, spli...  9.76 us
  transfers between devices with their start and end apart: 7, of which 5 were waited for; matrix products, arithmetic and copies ran while one was open for 16% of the time, Pallas kernels for 0%

profile of v1, /device:TPU:2, one launch (start us, length us, event | category | flops | bytes accessed | tf_op | source)
XLA Modules:
  0.0 322.7 jit_solution(4474217241358795864)
XLA Ops:
  10.9 1.4 scatter_custom_fusion
  13.5 1.3 fusion.17
  14.9 1.4 fusion.19
  16.3 3.0 gather_fusion
  19.3 2.4 gather.13
  21.9 1.6 broadcast_select_fusion.2
  23.5 12.1 %all-to-all-start = ((bf16[64,5,2048]{2,1,0:T(8,128)(2,1)}), bf16[64,5,2048]{2,1,0:T(8,128)(2,1)S(1)}, u32[]{:S(2)}, u32[]{:S(2)}) async-start(bf16[64,5,2048]{2,1,0:T(8,128)(2,1)} %broadcast_select_fusion.2), calls=%async_computation | async-start | bytes 4194304 | tf_op jit(solution)/shard_map/all_to_all | solution.py:194
  37.5 3.5 %collective-permute-start = (bf16[3,2048]{0,1:T(8,128)(2,1)}, bf16[3,2048]{0,1:T(8,128)(2,1)}, u32[]{:S(2)}, u32[]{:S(2)}) collective-permute-start(bf16[3,2048]{0,1:T(8,128)(2,1)} %copy.55), channel_id=1, source_target_pairs={{0,1},{1,2},{2,3},{3,4},{4,5},{5,6},{6,7},{7,8},{8,9},{9,10},{10,1... | collective-permute-start | bytes 36872 | tf_op jit(solution)/shard_map/ppermute | solution.py:34
  41.6 2.0 copy.56
  45.2 11.4 %collective-permute-done = bf16[3,2048]{0,1:T(8,128)(2,1)} collective-permute-done((bf16[3,2048]{0,1:T(8,128)(2,1)}, bf16[3,2048]{0,1:T(8,128)(2,1)}, u32[]{:S(2)}, u32[]{:S(2)}) %collective-permute-start) | collective-permute-done | bytes 12320 | tf_op jit(solution)/shard_map/ppermute | solution.py:34
  56.6 4.6 %add_convert_fusion = bf16[128,2048]{0,1:T(8,128)(2,1)S(1)} fusion(bf16[128,2048]{0,1:T(8,128)(2,1)} %copy.56, bf16[3,2048]{0,1:T(8,128)(2,1)} %collective-permute-done, f32[2048]{0:T(1024)S(1)} %bitcast.221, f32[2048]{0:T(1024)S(1)} %bitcast.222, f32[2048]{0:T(1024)S(1)} %bitcast.220, f32[2048]{0:T(1024)S(1)} %bitcast.219), kind=kLoop, calls=%fused_computation.61 | loop fusion | flops 5505024 | bytes 1093632 | tf_op jit(solution)/shard_map/convert_element_type | solution.py:88
  62.0 1.5 fusion.14
  63.4 2.5 copy.59
  66.0 1.8 copy.63
  67.8 19.0 %all-to-all-done = bf16[64,5,2048]{2,1,0:T(8,128)(2,1)S(1)} async-done(((bf16[64,5,2048]{2,1,0:T(8,128)(2,1)}), bf16[64,5,2048]{2,1,0:T(8,128)(2,1)S(1)}, u32[]{:S(2)}, u32[]{:S(2)}) %all-to-all-start) | async-done | bytes 1310752 | tf_op jit(solution)/shard_map/all_to_all | solution.py:194
  86.8 1.4 reshape.838
  88.2 1.6 collective-permute-start.1
  89.8 2.8 fusion.10
  92.7 1.5 copy.61
  94.2 3.0 fusion.27
  97.2 1.7 copy.62
  100.0 1.4 add_exponential_fusion
  101.4 2.0 collective-permute-start.2
  103.4 15.4 %collective-permute-done.1 = bf16[320,2048]{1,0:T(8,128)(2,1)} collective-permute-done((bf16[320,2048]{1,0:T(8,128)(2,1)}, bf16[320,2048]{1,0:T(8,128)(2,1)}, u32[]{:S(2)}, u32[]{:S(2)}) %collective-permute-start.1) | collective-permute-done | bytes 1310752 | tf_op jit(solution)/shard_map/ppermute | solution.py:21
  119.1 2.3 slice_add_fusion
  121.4 2.9 stack.4
  124.3 1.7 slice_multiply_fusion
  126.0 3.9 %stack.5 = f32[16,8,2048]{2,1,0:T(8,128)} concatenate(f32[16,1,2048]{2,1,0:T(1,128)} %get-tuple-element.108, f32[16,1,2048]{2,1,0:T(1,128)} %get-tuple-element.94, f32[16,1,2048]{2,1,0:T(1,128)} %get-tuple-element.93, f32[16,1,2048]{2,1,0:T(1,128)} %get-tuple-element.92, f32[16,1,2048]{2,1,0:T(1,128)} %get-tuple-element.91, f32[16,1,2048]{2,1,0:T(1,128)} %get-tuple-element.90, ...), dimensions={1} | concatenate | bytes 2097152 | tf_op jit(solution)/shard_map/stack | solution.py:115
  130.8 1.6 constant_dynamic-update-slice_fusion.2
  132.4 1.5 constant_dynamic-update-slice_fusion.1
  133.9 14.7 %collective-permute-done.3 = bf16[320,2048]{1,0:T(8,128)(2,1)} collective-permute-done((bf16[320,2048]{1,0:T(8,128)(2,1)}, bf16[320,2048]{1,0:T(8,128)(2,1)}, u32[]{:S(2)}, u32[]{:S(2)}) %collective-permute-start.3) | collective-permute-done | bytes 1310752 | tf_op jit(solution)/shard_map/ppermute | solution.py:21
  148.6 1.5 constant_dynamic-update-slice_fusion
  150.0 2.4 copy-done.2
  152.4 7.1 %fusion.5 = f32[1280,896]{1,0:T(8,128)} fusion(bf16[1280,2048]{1,0:T(8,128)(2,1)S(1)} %constant_dynamic-update-slice_fusion, bf16[1,2048,896]{2,1,0:T(8,128)(2,1)S(1)} %copy-done.16), kind=kOutput, calls=%fused_computation.13 | convolution fusion | flops 4697620480 | bytes 13500416 | tf_op jit(solution)/shard_map/dot_general | solution.py:149
  159.5 17.5 %convolution_convert_fusion = bf16[1280,2048]{1,0:T(8,128)(2,1)} fusion(bf16[1,896,2048]{2,1,0:T(8,128)(2,1)} %param.29, f32[1280,896]{1,0:T(8,128)} %fusion.5, bf16[1280,2048]{1,0:T(8,128)(2,1)} %copy-done.2, bf16[1,2048,896]{2,1,0:T(8,128)(2,1)} %param.28), kind=kOutput, calls=%fused_computation.8 | convolution fusion | flops 9404743680 | bytes 22413312 | tf_op jit(solution)/shard_map/dot_general | solution.py:199
  178.1 7.8 %while.17 = (s32[]{:T(128)}, f32[2048]{0:T(1024)S(1)}, f32[2048]{0:T(1024)S(1)}, f32[16,2048]{1,0:T(8,128)S(1)}, f32[16,2048]{1,0:T(8,128)S(1)}, /*index=5*/f32[...) while((s32[]{:T(128)}, f32[2048]{0:T(1024)S(1)}, f32[2048]{0:T(1024)S(1)}, ...), condition=%wide.region_1.2_spmd.clone, body=%wide.region_0.1_spmd.clone.sunk | while | flops 10243 | bytes 131187 | solution.py:122
  185.9 1.5 multiply_bitcast_fusion
  187.4 12.4 %all-gather.4 = f32[4,2,2048]{2,1,0:T(2,128)S(1)} all-gather(f32[1,2,2048]{2,1,0:T(2,128)S(1)} %maximum_bitcast_fusion), channel_id=2, replica_groups=mesh['ep_0'=8,'ep_1'=4,'ep_2'=2,'tp'=4] {'tp'}, dimensions={0}, use_global_device_ids=true | all-gather | bytes 81920 | tf_op jit(solution)/shard_map/all_gather | solution.py:51
  199.9 1.8 all-gather.5
  201.8 13.4 %all-gather.6 = f32[4,2,2048]{2,1,0:T(2,128)S(1)} all-gather(f32[1,2,2048]{2,1,0:T(2,128)S(1)} %maximum_bitcast_fusion.2), channel_id=4, replica_groups=mesh['ep_0'=8,'ep_1'=4,'ep_2'=2,'tp'=4] {'ep_1'}, dimensions={0}, use_global_device_ids=true | all-gather | bytes 81920 | tf_op jit(solution)/shard_map/all_gather | solution.py:51
  215.3 26.3 %all-gather.7 = f32[8,2,2048]{2,1,0:T(2,128)S(1)} all-gather(f32[1,2,2048]{2,1,0:T(2,128)S(1)} %maximum_bitcast_fusion.3), channel_id=5, replica_groups=mesh['ep_0'=8,'ep_1'=4,'ep_2'=2,'tp'=4] {'ep_0'}, dimensions={0}, use_global_device_ids=true | all-gather | bytes 147456 | tf_op jit(solution)/shard_map/all_gather | solution.py:51
  241.6 3.5 %reshape.839 = bf16[64,5,2048]{2,1,0:T(8,128)(2,1)} reshape(bf16[320,2048]{1,0:T(8,128)(2,1)} %reduce-scatter.2.cloned.1.call-done) | data formatting | bytes 2621440 | tf_op jit(solution)/shard_map/reshape | solution.py:205
  245.1 9.8 %all-to-all-start.1 = ((bf16[64,5,2048]{2,1,0:T(8,128)(2,1)}), bf16[64,5,2048]{2,1,0:T(8,128)(2,1)}, u32[]{:S(2)}, u32[]{:S(2)}) async-start(bf16[64,5,2048]{2,1,0:T(8,128)(2,1)} %reshape.839), calls=%async_computation.2 | async-start | bytes 4194304 | tf_op jit(solution)/shard_map/all_to_all | solution.py:204
  255.2 1.3 fusion.26
  256.4 49.6 %all-to-all-done.1 = bf16[64,5,2048]{2,1,0:T(8,128)(2,1)} async-done(((bf16[64,5,2048]{2,1,0:T(8,128)(2,1)}), bf16[64,5,2048]{2,1,0:T(8,128)(2,1)}, u32[]{:S(2)}, u32[]{:S(2)}) %all-to-all-start.1) | async-done | bytes 1310752 | tf_op jit(solution)/shard_map/all_to_all | solution.py:204
  306.0 2.6 reshape.840
  308.6 1.6 gather_fusion.1
  311.0 4.9 %multiply_reduce_fusion = bf16[128,2048]{1,0:T(8,128)(2,1)} fusion(bf16[128,2,2048]{2,1,0:T(2,128)(2,1)S(1)} %gather.15, pred[128,2]{1,0:T(8,128)(4,1)S(1)} %copy-done.11, f32[128,2]{1,0:T(8,128)S(1)} %copy-done.8), kind=kLoop, calls=%fused_computation.15 | loop fusion | flops 1835008 | bytes 1574144 | tf_op jit(solution)/shard_map/reduce_sum | solution.py:214
  (161 shorter events, 21.4 us)
Async XLA Ops:
  7.2 54.8 %copy-start = (bf16[8,256,256]{2,1,0:T(8,128)(2,1)S(1)}, bf16[8,256,256]{2,1,0:T(8,128)(2,1)}, u32[]{:S(2)}) copy-start(bf16[8,256,256]{2,1,0:T(8,128)(2,1)} %param.19) | copy-start | bytes 3145732
  21.8 19.1 %copy-start.13 = (f32[2048]{0:T(1024)S(1)}, f32[2048]{0:T(1024)}, u32[]{:S(2)}) copy-start(f32[2048]{0:T(1024)} %param.21) | copy-start | bytes 24580
  21.8 19.2 %copy-start.12 = (f32[4,2048]{1,0:T(4,128)S(1)}, f32[4,2048]{1,0:T(4,128)}, u32[]{:S(2)}) copy-start(f32[4,2048]{1,0:T(4,128)} %param.18) | copy-start | bytes 98308
  23.4 21.0 %copy-start.15 = (f32[128,2]{0,1:T(2,128)S(1)}, f32[128,2]{0,1:T(2,128)}, u32[]{:S(2)}) copy-start(f32[128,2]{0,1:T(2,128)} %param.25) | copy-start | bytes 3076
  23.5 21.7 %copy-start.14 = (f32[128]{0:T(128)S(1)}, f32[128]{0:T(128)}, u32[]{:S(2)}) copy-start(f32[128]{0:T(128)} %param.22) | copy-start | bytes 1540
  23.5 63.4 %all-to-all-start = ((bf16[64,5,2048]{2,1,0:T(8,128)(2,1)}), bf16[64,5,2048]{2,1,0:T(8,128)(2,1)S(1)}, u32[]{:S(2)}, u32[]{:S(2)}) async-start(bf16[64,5,2048]{2,1,0:T(8,128)(2,1)} %broadcast_select_fusion.2), calls=%async_computation | async-start | bytes 4194304 | tf_op jit(solution)/shard_map/all_to_all | solution.py:194
  35.6 206.0 %reduce-scatter.2.cloned.1.call-start = ((), (), s32[]{:S(2)}) async-start(), calls=%async_computation.3 | async-start | bytes 6553600 | tf_op jit(solution)/shard_map/reduce_scatter | solution.py:198
  37.5 19.1 %collective-permute-start = (bf16[3,2048]{0,1:T(8,128)(2,1)}, bf16[3,2048]{0,1:T(8,128)(2,1)}, u32[]{:S(2)}, u32[]{:S(2)}) collective-permute-start(bf16[3,2048]{0,1:T(8,128)(2,1)} %copy.55), channel_id=1, source_target_pairs={{0,1},{1,2},{2,3},{3,4},{4,5},{5,6},{6,7},{7,8},{8,9},{9,10},{10,1... | collective-permute-start | bytes 36872 | tf_op jit(solution)/shard_map/ppermute | solution.py:34
  61.2 0.8 copy-start.5
  88.2 6.0 %copy-start.4 = (f32[128,8,256]{0,2,1:T(8,128)S(1)}, f32[128,8,256]{0,2,1:T(8,128)}, u32[]{:S(2)}) copy-start(f32[128,8,256]{0,2,1:T(8,128)} %copy.59) | copy-start | bytes 3145732
  88.2 30.6 %collective-permute-start.1 = (bf16[320,2048]{1,0:T(8,128)(2,1)}, bf16[320,2048]{1,0:T(8,128)(2,1)}, u32[]{:S(2)}, u32[]{:S(2)}) collective-permute-start(bf16[320,2048]{1,0:T(8,128)(2,1)} %reshape.838), channel_id=1, source_target_pairs={{0,1},{1,2},{2,3},{3,0},{4,5},{5,6},{6,7},{7,4},{8,9},{9,10},{10,1... | collective-permute-start | bytes 3932168 | tf_op jit(solution)/shard_map/ppermute | solution.py:21
  97.2 4.2 %copy-start.3 = (bf16[320,2048]{1,0:T(8,128)(2,1)S(1)}, bf16[320,2048]{1,0:T(8,128)(2,1)}, u32[]{:S(2)}) copy-start(bf16[320,2048]{1,0:T(8,128)(2,1)} %reshape.838) | copy-start | bytes 3932164
  101.4 30.9 %collective-permute-start.2 = (bf16[320,2048]{1,0:T(8,128)(2,1)S(1)}, bf16[320,2048]{1,0:T(8,128)(2,1)}, u32[]{:S(2)}, u32[]{:S(2)}) collective-permute-start(bf16[320,2048]{1,0:T(8,128)(2,1)S(1)} %copy-done.3), channel_id=1, source_target_pairs={{0,3},{1,0},{2,1},{3,2},{4,7},{5,4},{6,5},{7,6},{8,11},{9,8},{10,9... | collective-permute-start | bytes 3932168 | tf_op jit(solution)/shard_map/ppermute | solution.py:24
  118.8 29.7 %collective-permute-start.3 = (bf16[320,2048]{1,0:T(8,128)(2,1)}, bf16[320,2048]{1,0:T(8,128)(2,1)}, u32[]{:S(2)}, u32[]{:S(2)}) collective-permute-start(bf16[320,2048]{1,0:T(8,128)(2,1)} %collective-permute-done.1), channel_id=1, source_target_pairs={{0,1},{1,2},{2,3},{3,0},{4,5},{5,6},{6,7},{7,4},{8,9},{9,10},{10,1... | collective-permute-start | bytes 3932168 | tf_op jit(solution)/shard_map/ppermute | solution.py:21
  130.7 21.6 %copy-start.16 = (bf16[1,2048,896]{2,1,0:T(8,128)(2,1)S(1)}, bf16[1,2048,896]{2,1,0:T(8,128)(2,1)}, u32[]{:S(2)}) copy-start(bf16[1,2048,896]{2,1,0:T(8,128)(2,1)} %param.27) | copy-start | bytes 11010052
  150.0 2.4 copy-start.2
  177.1 0.9 copy-start.6
  177.1 1.0 copy-start.9
  177.1 1.0 copy-start.10
  241.6 13.6 %copy-start.7 = (bf16[128,2048]{1,0:T(8,128)(2,1)S(1)}, bf16[128,2048]{1,0:T(8,128)(2,1)}, u32[]{:S(2)}) copy-start(bf16[128,2048]{1,0:T(8,128)(2,1)} %param.16) | copy-start | bytes 1572868
  245.1 60.9 %all-to-all-start.1 = ((bf16[64,5,2048]{2,1,0:T(8,128)(2,1)}), bf16[64,5,2048]{2,1,0:T(8,128)(2,1)}, u32[]{:S(2)}, u32[]{:S(2)}) async-start(bf16[64,5,2048]{2,1,0:T(8,128)(2,1)} %reshape.839), calls=%async_computation.2 | async-start | bytes 4194304 | tf_op jit(solution)/shard_map/all_to_all | solution.py:204
  308.5 2.4 copy-start.8
  308.6 2.4 copy-start.11
  308.6 7.3 %copy-start.1 = (bf16[8,256,256]{2,1,0:T(8,128)(2,1)S(1)}, bf16[8,256,256]{2,1,0:T(8,128)(2,1)}, u32[]{:S(2)}) copy-start(bf16[8,256,256]{2,1,0:T(8,128)(2,1)} %param.19) | copy-start | bytes 3145732
Sparse Core Ops, SparseCore 0:
  177.2 58.1 reduce-scatter.1
